TPU v7x, 32 devices: a whole 2x2x4 slice. The times are simulated.
32 devices in a mesh: sp: 8 (over z, x), tp: 4 (over y, core).
Axes of the slice: x: 2, y: 2, z: 4, core: 2. Of those that a mesh axis runs over, the one named last changes fastest.
Arguments:
- residual: bfloat16 [4096, 2048], P(('sp', 'tp')), may hold values from -6 to 6
- query_small: bfloat16 [4096, 8, 128], P('sp', 'tp'), may hold values from -120 to 120
- key_small: bfloat16 [4096, 8, 128], P('sp', 'tp'), may hold values from -6 to 6
- value_small: bfloat16 [4096, 8, 128], P('sp', 'tp'), may hold values from -6 to 6
- query_large: bfloat16 [4096, 8, 256], P('sp', 'tp'), may hold values from -120 to 120
- key_large: bfloat16 [4096, 8, 256], P('sp', 'tp'), may hold values from -6 to 6
- value_large: bfloat16 [4096, 8, 128], P('sp', 'tp'), may hold values from -6 to 6
- lambda_small: float32 [8], P('tp'), may hold values from 0.3 to 0.8
- lambda_large: float32 [8], P('tp'), may hold values from 0.3 to 0.8
- head_gain: float32 [128], replicated, may hold values from 0.1 to 1.9
- output_small: bfloat16 [1024, 2048], P('tp'), may hold values from -0.125 to 0.125
- output_large: bfloat16 [1024, 2048], P('tp'), may hold values from -0.125 to 0.125
- norm_gain: float32 [2048], replicated, may hold values from 0.1 to 1.9
- gate_weight: bfloat16 [2048, 5632], P('sp', 'tp'), may hold values from -0.125 to 0.125
- up_weight: bfloat16 [2048, 5632], P('sp', 'tp'), may hold values from -0.125 to 0.125
- down_weight: bfloat16 [5632, 2048], P('tp', 'sp'), may hold values from -0.3125 to 0.3125
Outputs:
- block_output: bfloat16 [4096, 2048], P(('sp', 'tp'))
All inputs are finite; a program needn't handle non-finite values.
Results may differ from a plain program's by a relative error of at most 0.015.
Values may be sent and summed in bfloat16 or wider, within the bound.
No kernel may reach another device: no remote copies, remote signals or barrier semaphores. Data moves between devices by JAX's collectives and lax.ppermute only.
A program may use at most 128 MiB of HBM per device.

v0:
```python
import math
import jax
import jax.numpy as jnp
from jax import lax
from jax.sharding import PartitionSpec as P

residual_scale = 8.0**0.25
branch_scale = 0.8
norm_epsilon = 1e-05
masked_score = -1e30


def from_partner(value, axis, distance):
    mask = 2**distance
    pairs = [(source, source ^ mask) for source in range(lax.axis_size(axis))]
    return lax.ppermute(value, axis, pairs)


def layer_norm(values, gains):
    centered = values - jnp.mean(values, axis=-1, keepdims=True)
    variance = jnp.mean(centered * centered, axis=-1, keepdims=True)
    return centered * lax.rsqrt(variance + norm_epsilon) * gains


def empty_state(head_count, tokens, width):
    return (
        jnp.full((head_count, 2, tokens), masked_score, jnp.float32),
        jnp.zeros((head_count, 2, tokens), jnp.float32),
        jnp.zeros((head_count, 2, tokens, width), jnp.float32),
    )


def absorb_group(state, query_maps, key_block, value_block, key_index, query_index):
    running_max, totals, accumulated = state
    head_size = query_maps.shape[3]
    scores = jnp.einsum(
        "qhmd,khmd->hmqk", query_maps, key_block, preferred_element_type=jnp.float32
    ) * head_size ** (-0.5)
    visible = key_index[None, :] <= query_index[:, None]
    scores = jnp.where(visible, scores, masked_score)
    new_max = jnp.maximum(running_max, jnp.max(scores, axis=-1))
    fading = jnp.exp(running_max - new_max)
    weights = jnp.where(visible, jnp.exp(scores - new_max[..., None]), 0.0)
    totals = totals * fading + jnp.sum(weights, axis=-1)
    accumulated = accumulated * fading[..., None] + jnp.einsum(
        "hmqk,khe->hmqe",
        weights.astype(jnp.bfloat16),
        value_block,
        preferred_element_type=jnp.float32,
    )
    return (new_max, totals, accumulated)


def finish_group(state, lambdas, head_gain):
    running_max, totals, accumulated = state
    map_out = accumulated / totals[..., None]
    combined = map_out[:, 0] - lambdas[:, None, None] * map_out[:, 1]
    mean_square = jnp.mean(combined * combined, axis=-1, keepdims=True)
    normed = (combined * lax.rsqrt(mean_square + norm_epsilon) * head_gain * branch_scale).astype(
        jnp.bfloat16
    )
    head_count, tokens, width = normed.shape
    return jnp.transpose(normed, (1, 0, 2)).reshape(tokens, head_count * width)


def per_device(
    residual,
    query_small,
    key_small,
    value_small,
    query_large,
    key_large,
    value_large,
    lambda_small,
    lambda_large,
    head_gain,
    output_small,
    output_large,
    norm_gain,
    gate_weight,
    up_weight,
    down_weight,
):
    tokens = query_small.shape[0]
    half = tokens // 2
    own_rows = residual.shape[0]
    bit_count = lax.axis_size("sp").bit_length() - 1
    residual_all = lax.all_gather(residual, "tp", axis=0, tiled=True)
    heads_small = query_small.shape[1]
    heads_large = query_large.shape[1]
    value_width = value_small.shape[2]
    first_start = lax.axis_index("sp") * tokens
    later_small = query_small[half:]
    later_large = query_large[half:]
    for bit in range(bit_count):
        later_small, later_large = from_partner((later_small, later_large), "sp", bit)
    second_start = (lax.axis_size("sp") - 1 - lax.axis_index("sp")) * tokens + half
    halves = (
        (
            query_small[:half].reshape(half, heads_small, 2, -1),
            query_large[:half].reshape(half, heads_large, 2, -1),
            first_start + jnp.arange(half, dtype=jnp.int32),
        ),
        (
            later_small.reshape(half, heads_small, 2, -1),
            later_large.reshape(half, heads_large, 2, -1),
            second_start + jnp.arange(half, dtype=jnp.int32),
        ),
    )
    one_half = (
        empty_state(heads_small, half, value_width),
        empty_state(heads_large, half, value_width),
    )
    keys_first = lax.all_gather(key_small, "sp", axis=0, tiled=True)
    keys_second = lax.all_gather(key_large, "sp", axis=0, tiled=True)
    values_first = lax.all_gather(value_small, "sp", axis=0, tiled=True)
    values_second = lax.all_gather(value_large, "sp", axis=0, tiled=True)
    row_count = keys_first.shape[0]
    block_size = math.gcd(row_count, 512)
    number = row_count // block_size
    stacked = (
        keys_first.reshape(number, block_size, heads_small, 2, -1),
        keys_second.reshape(number, block_size, heads_large, 2, -1),
        values_first.reshape(number, block_size, heads_small, value_width),
        values_second.reshape(number, block_size, heads_large, value_width),
    )

    def step(carried, block_items):
        block_index, blocks = block_items
        key_index = block_index * block_size + jnp.arange(block_size, dtype=jnp.int32)
        updated = []
        for which in range(2):
            maps_small, maps_large, query_index = halves[which]

            def take(pair):
                return (
                    absorb_group(pair[0], maps_small, blocks[0], blocks[2], key_index, query_index),
                    absorb_group(pair[1], maps_large, blocks[1], blocks[3], key_index, query_index),
                )

            def leave(pair):
                return pair

            updated.append(
                lax.cond(key_index[0] <= query_index[half - 1], take, leave, carried[which])
            )
        return ((updated[0], updated[1]), None)

    result, unused = lax.scan(
        step, (one_half, one_half), (jnp.arange(number, dtype=jnp.int32), stacked)
    )
    first_states, second_states = result
    early_small = finish_group(first_states[0], lambda_small, head_gain)
    early_large = finish_group(first_states[1], lambda_large, head_gain)
    late_small = finish_group(second_states[0], lambda_small, head_gain)
    late_large = finish_group(second_states[1], lambda_large, head_gain)
    for bit in range(bit_count):
        late_small, late_large = from_partner((late_small, late_large), "sp", bit)
    attended_small = jnp.concatenate([early_small, late_small], axis=0)
    attended_large = jnp.concatenate([early_large, late_large], axis=0)
    mixed_sum = lax.psum(
        (
            jnp.dot(attended_small, output_small, preferred_element_type=jnp.float32)
            + jnp.dot(attended_large, output_large, preferred_element_type=jnp.float32)
        ).astype(jnp.bfloat16),
        "tp",
    ).astype(jnp.float32)
    whole_rows = layer_norm(
        residual_scale * residual_all.astype(jnp.float32) + mixed_sum, norm_gain
    ).astype(jnp.bfloat16)
    normed = lax.dynamic_slice_in_dim(whole_rows, lax.axis_index("tp") * own_rows, own_rows, 0)
    gate_rows = jnp.dot(
        whole_rows,
        lax.all_gather(gate_weight, "sp", axis=0, tiled=True),
        preferred_element_type=jnp.float32,
    )
    up_rows = jnp.dot(
        whole_rows,
        lax.all_gather(up_weight, "sp", axis=0, tiled=True),
        preferred_element_type=jnp.float32,
    )
    down_full = lax.all_gather(down_weight, "sp", axis=1, tiled=True)
    hidden = (jax.nn.silu(gate_rows) * up_rows).astype(jnp.bfloat16)
    down_sum = lax.psum_scatter(
        jnp.dot(hidden, down_full, preferred_element_type=jnp.float32).astype(jnp.bfloat16),
        "tp",
        scatter_dimension=0,
        tiled=True,
    ).astype(jnp.float32)
    return (residual_scale * normed.astype(jnp.float32) + 0.5 * down_sum).astype(jnp.bfloat16)


def solution(mesh):
    in_specs = (
        P(("sp", "tp"), None),
        P("sp", "tp", None),
        P("sp", "tp", None),
        P("sp", "tp", None),
        P("sp", "tp", None),
        P("sp", "tp", None),
        P("sp", "tp", None),
        P("tp"),
        P("tp"),
        P(),
        P("tp", None),
        P("tp", None),
        P(),
        P("sp", "tp"),
        P("sp", "tp"),
        P("tp", "sp"),
    )
    out_specs = P(("sp", "tp"), None)
    return jax.shard_map(
        per_device, mesh=mesh, in_specs=in_specs, out_specs=out_specs, check_vma=False
    )
```

profile of v0, /device:TPU:0, one launch (start us, length us, event | category | flops | bytes accessed | tf_op | source)
XLA Modules:
  0.0 791.7 jit_solution(11565010698791997182)
XLA Ops:
  12.2 3.0 collective-permute-start.3
  15.2 6.3 collective-permute-done.3
  25.1 3.5 collective-permute-done
  30.0 7.0 collective-permute-done.4
  43.6 29.2 %collective-permute-done.2 = bf16[256,2,128]{2,1,0:T(2,128)(2,1)S(1)} collective-permute-done((bf16[256,2,128]{2,1,0:T(2,128)(2,1)S(1)}, bf16[256,2,128]{2,1,0:T(2,128)(2,1)S(1)}, u32[]{:S(2)}, u32[]{:S(2)}) %collective-permute-start.2) | collective-permute-done | bytes 131104 | tf_op jit(solution)/shard_map/ppermute | solution.py:16
  73.8 9.7 %reshape.126 = bf16[8,512,2,2,64]{4,3,2,1,0:T(2,128)(2,1)} reshape(bf16[4096,2,128]{2,1,0:T(2,128)(2,1)} %all-gather.11.cloned.1.call-done) | data formatting | bytes 4194304 | tf_op jit(solution)/shard_map/reshape | solution.py:122
  83.5 10.6 %copy.56 = bf16[8,512,2,2,64]{1,4,3,2,0:T(8,128)(2,1)} copy(bf16[8,512,2,2,64]{4,3,2,1,0:T(2,128)(2,1)} %reshape.126) | data formatting | bytes 4194304 | tf_op jit(solution)/shard_map/while | solution.py:149
  94.1 54.6 %all-gather.15.cloned.1.call-done = bf16[4096,2,256]{2,1,0:T(2,128)(2,1)} async-done(((bf16[512,2,256]{2,1,0:T(2,128)(2,1)}), bf16[4096,2,256]{2,1,0:T(2,128)(2,1)}) %all-gather.15.cloned.1.call-update) | async-done | bytes 4194320 | tf_op jit(solution)/shard_map/all_gather | solution.py:115
  148.7 11.7 %reshape.127 = bf16[8,512,2,2,128]{4,3,2,1,0:T(2,128)(2,1)} reshape(bf16[4096,2,256]{2,1,0:T(2,128)(2,1)} %all-gather.15.cloned.1.call-done) | data formatting | bytes 8388608 | tf_op jit(solution)/shard_map/reshape | solution.py:123
  160.4 38.1 %all-gather.13.cloned.1.call-done = bf16[4096,2,128]{2,0,1:T(8,128)(2,1)} async-done(((bf16[512,2,128]{2,0,1:T(8,128)(2,1)}), bf16[4096,2,128]{2,0,1:T(8,128)(2,1)}) %all-gather.13.cloned.1.call-update) | async-done | bytes 2097168 | tf_op jit(solution)/shard_map/all_gather | solution.py:116
  198.5 49.7 %all-gather.17.cloned.1.call-done = bf16[4096,2,128]{2,0,1:T(8,128)(2,1)} async-done(((bf16[512,2,128]{2,0,1:T(8,128)(2,1)}), bf16[4096,2,128]{2,0,1:T(8,128)(2,1)}) %all-gather.17.cloned.1.call-update) | async-done | bytes 2097168 | tf_op jit(solution)/shard_map/all_gather | solution.py:117
  251.6 124.7 %while.32 = (s32[]{:T(128)}, f32[2,2,256]{2,1,0:T(2,128)S(1)}, f32[2,2,256]{2,1,0:T(2,128)S(1)}, f32[2,2,256,128]{3,2,1,0:T(8,128)}, f32[2,2,256]{2,1,0:T(2,128)...) while((s32[]{:T(128)}, f32[2,2,256]{2,1,0:T(2,128)S(1)}, ...), condition=%wide.region_13.14_spmd, body=%wide.region_0.13_spmd.sunk | while | flops 968106496 | bytes 58991568 | solution.py:149
  258.8 5.7 conditional.5
  266.5 5.8 conditional.4
  279.4 5.7 conditional.5
  294.2 5.7 conditional.5
  309.1 5.7 conditional.5
  323.9 5.7 conditional.5
  338.8 5.7 conditional.5
  353.6 5.7 conditional.5
  368.4 5.7 conditional.5
  386.6 2.9 collective-permute-done.9
  394.7 3.6 collective-permute-start.11
  398.3 2.8 collective-permute-start.8
  410.6 48.7 %all-reduce.2.cloned.1.call-done = bf16[512,2048]{1,0:T(8,128)(2,1)} async-done(((bf16[512,2048]{1,0:T(8,128)(2,1)}), bf16[512,2048]{1,0:T(8,128)(2,1)}) %all-reduce.2.cloned.1.call-update) | async-done | bytes 2097168 | tf_op jit(solution)/shard_map/psum | solution.py:161
  459.3 3.1 fusion.48
  465.9 88.0 %all-gather.19.cloned.1.call-done = bf16[2048,1408]{1,0:T(8,128)(2,1)} async-done(((bf16[256,1408]{1,0:T(8,128)(2,1)}), bf16[2048,1408]{1,0:T(8,128)(2,1)}) %all-gather.19.cloned.1.call-update) | async-done | bytes 5767184 | tf_op jit(solution)/shard_map/all_gather | solution.py:174
  553.9 8.2 %fusion.72 = f32[512,1408]{1,0:T(8,128)} fusion(bf16[512,2048]{1,0:T(8,128)(2,1)} %multiply_convert_fusion, bf16[2048,1408]{1,0:T(8,128)(2,1)} %all-gather.19.cloned.1.call-done), kind=kOutput, calls=%fused_computation.131 | convolution fusion | flops 2952790016 | bytes 10747904 | tf_op jit(solution)/shard_map/dot_general | solution.py:172
  562.1 84.5 %all-gather.21.cloned.1.call-done = bf16[2048,1408]{1,0:T(8,128)(2,1)} async-done(((bf16[256,1408]{1,0:T(8,128)(2,1)}), bf16[2048,1408]{1,0:T(8,128)(2,1)}) %all-gather.21.cloned.1.call-update) | async-done | bytes 5767184 | tf_op jit(solution)/shard_map/all_gather | solution.py:179
  646.6 93.4 %all-gather.23.cloned.1.call-done = bf16[1408,2048]{1,0:T(8,128)(2,1)} async-done(((bf16[1408,256]{1,0:T(8,128)(2,1)}), bf16[1408,2048]{1,0:T(8,128)(2,1)}) %all-gather.23.cloned.1.call-update) | async-done | bytes 5767184 | tf_op jit(solution)/shard_map/all_gather | solution.py:182
  740.0 13.3 %convolution_convert_fusion = bf16[512,2048]{1,0:T(8,128)(2,1)} fusion(bf16[1408,2048]{1,0:T(8,128)(2,1)} %all-gather.23.cloned.1.call-done, bf16[512,2048]{1,0:T(8,128)(2,1)S(1)} %copy-done.3, bf16[2048,1408]{1,0:T(8,128)(2,1)} %all-gather.21.cloned.1.call-done, f32[512,1408]{1,0:T(8,128)} %fusion.72), kind=kOutput, calls=%fused_computation.79 | convolution fusion | flops 5910953984 | bytes 18612224 | tf_op jit(solution)/shard_map/dot_general | solution.py:185
  753.3 29.5 %reduce-scatter.2.cloned.1.call-done = bf16[128,2048]{1,0:T(8,128)(2,1)} async-done(((bf16[512,2048]{1,0:T(8,128)(2,1)}), bf16[128,2048]{1,0:T(8,128)(2,1)}) %reduce-scatter.2.cloned.1.call-update) | async-done | bytes 524304 | tf_op jit(solution)/shard_map/reduce_scatter | solution.py:184
  (368 shorter events, 150.1 us)
Async XLA Ops:
  6.5 396.8 %copy-start = (bf16[256,2048]{1,0:T(8,128)(2,1)S(1)}, bf16[256,2048]{1,0:T(8,128)(2,1)}, u32[]{:S(2)}) copy-start(bf16[256,2048]{1,0:T(8,128)(2,1)} %param.33) | copy-start | bytes 3145732
  6.5 5.1 copy-start.17
  6.5 16.8 %copy-start.18 = (bf16[512,2,128]{2,1,0:T(2,128)(2,1)S(1)}, bf16[512,2,128]{2,1,0:T(2,128)(2,1)}, u32[]{:S(2)}) copy-start(bf16[512,2,128]{2,1,0:T(2,128)(2,1)} %param.23) | copy-start | bytes 786436
  6.5 67.3 %all-gather.11.cloned.1.call-start = ((), (), s32[]{:S(2)}) async-start(), calls=%async_computation.2 | async-start | bytes 2359296 | tf_op jit(solution)/shard_map/all_gather | solution.py:114
  7.3 141.4 %all-gather.15.cloned.1.call-start = ((), (), s32[]{:S(2)}) async-start(), calls=%async_computation.4 | async-start | bytes 4718592 | tf_op jit(solution)/shard_map/all_gather | solution.py:115
  8.0 190.5 %all-gather.13.cloned.1.call-start = ((), (), s32[]{:S(2)}) async-start(), calls=%async_computation.3 | async-start | bytes 2359296 | tf_op jit(solution)/shard_map/all_gather | solution.py:116
  9.8 238.4 %all-gather.17.cloned.1.call-start = ((), (), s32[]{:S(2)}) async-start(), calls=%async_computation.5 | async-start | bytes 2359296 | tf_op jit(solution)/shard_map/all_gather | solution.py:117
  11.5 399.0 %all-gather.9.cloned.1.call-start = ((), (), s32[]{:S(2)}) async-start(), calls=%async_computation.1 | async-start | bytes 2621440 | tf_op jit(solution)/shard_map/all_gather | solution.py:88
  12.2 9.3 %collective-permute-start.3 = (bf16[256,2,256]{0,2,1:T(8,128)(2,1)S(1)}, bf16[256,2,256]{0,2,1:T(8,128)(2,1)S(1)}, u32[]{:S(2)}, u32[]{:S(2)}) collective-permute-start(bf16[256,2,256]{0,2,1:T(8,128)(2,1)S(1)} %copy.82), channel_id=1, source_target_pairs={{0,4},{4,0},{8,12},{12,8},{16,20},{20,16},{24,28},{28,24},{1,5},{5... | collective-permute-start | bytes 786440 | tf_op jit(solution)/shard_map/ppermute | solution.py:16
  21.5 15.5 %collective-permute-start.4 = (bf16[256,2,256]{0,2,1:T(8,128)(2,1)S(1)}, bf16[256,2,256]{0,2,1:T(8,128)(2,1)S(1)}, u32[]{:S(2)}, u32[]{:S(2)}) collective-permute-start(bf16[256,2,256]{0,2,1:T(8,128)(2,1)S(1)} %collective-permute-done.3), channel_id=1, source_target_pairs={{0,8},{4,12},{8,0},{12,4},{16,24},{20,28},{24,16},{28,20},{1,9},{5... | collective-permute-start | bytes 786440 | tf_op jit(solution)/shard_map/ppermute | solution.py:16
  23.5 5.0 collective-permute-start
  28.5 12.9 %collective-permute-start.1 = (bf16[256,2,128]{2,1,0:T(2,128)(2,1)S(1)}, bf16[256,2,128]{2,1,0:T(2,128)(2,1)S(1)}, u32[]{:S(2)}, u32[]{:S(2)}) collective-permute-start(bf16[256,2,128]{2,1,0:T(2,128)(2,1)S(1)} %collective-permute-done), channel_id=1, source_target_pairs={{0,8},{4,12},{8,0},{12,4},{16,24},{20,28},{24,16},{28,20},{1,9},{5... | collective-permute-start | bytes 393224 | tf_op jit(solution)/shard_map/ppermute | solution.py:16
  37.0 35.9 %collective-permute-start.5 = (bf16[256,2,256]{0,2,1:T(8,128)(2,1)S(1)}, bf16[256,2,256]{0,2,1:T(8,128)(2,1)S(1)}, u32[]{:S(2)}, u32[]{:S(2)}) collective-permute-start(bf16[256,2,256]{0,2,1:T(8,128)(2,1)S(1)} %collective-permute-done.4), channel_id=1, source_target_pairs={{0,16},{4,20},{8,24},{12,28},{16,0},{20,4},{24,8},{28,12},{1,17},{... | collective-permute-start | bytes 786440 | tf_op jit(solution)/shard_map/ppermute | solution.py:16
  41.5 31.3 %collective-permute-start.2 = (bf16[256,2,128]{2,1,0:T(2,128)(2,1)S(1)}, bf16[256,2,128]{2,1,0:T(2,128)(2,1)S(1)}, u32[]{:S(2)}, u32[]{:S(2)}) collective-permute-start(bf16[256,2,128]{2,1,0:T(2,128)(2,1)S(1)} %collective-permute-done.1), channel_id=1, source_target_pairs={{0,16},{4,20},{8,24},{12,28},{16,0},{20,4},{24,8},{28,12},{1,17},{... | collective-permute-start | bytes 393224 | tf_op jit(solution)/shard_map/ppermute | solution.py:16
  43.0 416.3 %all-reduce.2.cloned.1.call-start = ((), (), s32[]{:S(2)}) async-start(), calls=%async_computation.6 | async-start | bytes 4194304 | tf_op jit(solution)/shard_map/psum | solution.py:161
  376.3 4.6 copy-start.11
  377.7 4.3 copy-start.6
  379.8 3.2 copy-start.21
  384.5 5.0 collective-permute-start.9
  385.1 6.5 collective-permute-start.6
  389.6 5.1 collective-permute-start.10
  391.6 6.7 collective-permute-start.7
  394.7 8.6 %collective-permute-start.11 = (bf16[256,256]{0,1:T(8,128)(2,1)S(1)}, bf16[256,256]{0,1:T(8,128)(2,1)S(1)}, u32[]{:S(2)}, u32[]{:S(2)}) collective-permute-start(bf16[256,256]{0,1:T(8,128)(2,1)S(1)} %collective-permute-done.10), channel_id=1, source_target_pairs={{0,16},{4,20},{8,24},{12,28},{16,0},{20,4},{24,8},{28,12},{1,17},{... | collective-permute-start | bytes 393224 | tf_op jit(solution)/shard_map/ppermute | solution.py:16
  398.3 7.9 collective-permute-start.8
  403.3 2.8 copy-start.16
  408.3 145.6 %all-gather.19.cloned.1.call-start = ((), (), s32[]{:S(2)}) async-start(), calls=%async_computation.7 | async-start | bytes 6488064 | tf_op jit(solution)/shard_map/all_gather | solution.py:174
  409.0 237.6 %all-gather.21.cloned.1.call-start = ((), (), s32[]{:S(2)}) async-start(), calls=%async_computation.8 | async-start | bytes 6488064 | tf_op jit(solution)/shard_map/all_gather | solution.py:179
  409.8 330.2 %all-gather.23.cloned.1.call-start = ((), (), s32[]{:S(2)}) async-start(), calls=%async_computation.9 | async-start | bytes 6488064 | tf_op jit(solution)/shard_map/all_gather | solution.py:182
  410.5 372.3 %reduce-scatter.2.cloned.1.call-start = ((), (), s32[]{:S(2)}) async-start(), calls=%async_computation.10 | async-start | bytes 2621440 | tf_op jit(solution)/shard_map/reduce_scatter | solution.py:184
  410.6 51.9 %copy-start.1 = (bf16[512,2048]{1,0:T(8,128)(2,1)S(1)}, bf16[512,2048]{1,0:T(8,128)(2,1)}, u32[]{:S(2)}) copy-start(bf16[512,2048]{1,0:T(8,128)(2,1)} %all-gather.9.cloned.1.call-done) | copy-start | bytes 6291460
  459.3 3.1 copy-start.2
  465.9 274.1 %copy-start.3 = (bf16[512,2048]{1,0:T(8,128)(2,1)S(1)}, bf16[512,2048]{1,0:T(8,128)(2,1)}, u32[]{:S(2)}) copy-start(bf16[512,2048]{1,0:T(8,128)(2,1)} %multiply_convert_fusion) | copy-start | bytes 6291460
  (41 other events, 45.9 us)
Sparse Core Ops, SparseCore 0:
  9.5 64.2 all-gather.10
  75.9 72.7 all-gather.14
  150.9 47.5 all-gather.12
  200.6 47.5 all-gather.16
  249.6 21.0 all-gather.8
  408.4 50.8 all-reduce.1
  461.5 92.3 all-gather.18
  556.1 90.4 all-gather.20
  648.7 91.2 all-gather.22
  753.4 29.3 reduce-scatter.1
where the time goes:
time: 794 us; the launch traced here: 792 us
  waiting for transfers between devices  548 us (69%)
  local copies, waits for them, and re-layouts  102 us (13%)
  matrix products  52.3 us (7%)
  loops' own time  26.4 us (3%)
  other arithmetic  25.5 us (3%)
  starting transfers between devices  23.7 us (3%)
  between operations  13.9 us (2%)
    all_gather x1, waiting for transfers between devices, per_device(): down_full = lax.all_gather(down_weight, 'sp', axis=1, tiled=True)  93.4 us
    all_gather x1, waiting for transfers between devices, per_device(): lax.all_gather(gate_weight, 'sp', axis=0, tiled=True)  88 us
    all_gather x1, waiting for transfers between devices, per_device(): lax.all_gather(up_weight, 'sp', axis=0, tiled=True)  84.5 us
    ppermute x12, waiting for transfers between devices, from_partner(): return lax.ppermute(value, axis, pairs)  57.4 us
    all_gather x1, waiting for transfers between devices, per_device(): keys_second = lax.all_gather(key_large, 'sp', axis=0, tiled=True)  54.6 us
    all_gather x1, waiting for transfers between devices, per_device(): values_second = lax.all_gather(value_large, 'sp', axis=0, tiled=True)  49.7 us
    psum x1, waiting for transfers between devices, per_device(): lax.psum((jnp.dot(attended_small, output_small, preferred_element_type=jn...  48.7 us
    all_gather x1, waiting for transfers between devices, per_device(): values_first = lax.all_gather(value_small, 'sp', axis=0, tiled=True)  38.1 us
  transfers between devices with their start and end apart: 22, of which 18 were waited for; matrix products, arithmetic and copies ran while one was open for 20% of the time, Pallas kernels for 0%

commit v1 on v0

--- a/solution.py
+++ b/solution.py
@@ -114,7 +114,12 @@
     keys_first = lax.all_gather(key_small, "sp", axis=0, tiled=True)
     keys_second = lax.all_gather(key_large, "sp", axis=0, tiled=True)
     values_first = lax.all_gather(value_small, "sp", axis=0, tiled=True)
-    values_second = lax.all_gather(value_large, "sp", axis=0, tiled=True)
+    ring = [value_large]
+    for hop in range(7):
+        ring.append(lax.ppermute(ring[-1], "sp", [(dev, (dev + 1) % 8) for dev in range(8)]))
+    values_second = jnp.roll(
+        jnp.concatenate(ring[::-1], axis=0), (lax.axis_index("sp") + 1) * ring[0].shape[0], axis=0
+    )
     row_count = keys_first.shape[0]
     block_size = math.gcd(row_count, 512)
     number = row_count // block_size

time: 794 us -> 769 us (0.969)
  waiting for transfers between devices: 548 us -> 520 us
  local copies, waits for them, and re-layouts: 102 us -> 110 us
    ppermute x0 -> x7, waiting for transfers between devices: none -> 57.8 us  [per_device(): lax.ppermute(ring[-1], 'sp', [(dev, (dev + 1) % 8) for dev in range(8)])]
    all_gather x1 -> x0, waiting for transfers between devices: 49.7 us -> none  [per_device(): values_second = lax.all_gather(value_large, 'sp', axis=0, tiled=True)]
    all_gather x1, waiting for transfers between devices: 54.6 us -> 28.9 us  [per_device(): keys_second = lax.all_gather(key_large, 'sp', axis=0, tiled=True)]
    ppermute x12, starting transfers between devices: 23.3 us -> 14.2 us  [from_partner(): return lax.ppermute(value, axis, pairs)]
    ppermute x12, waiting for transfers between devices: 57.4 us -> 48.5 us  [from_partner(): return lax.ppermute(value, axis, pairs)]
  transfers between devices with their start and end apart: 22 -> 28, of which waited for: 18 -> 22; matrix products, arithmetic and copies ran while one was open for 20% -> 21% of each run, Pallas kernels for 0% -> 0%
where the time goes in v1:
time: 769 us; the launch traced here: 766 us
  waiting for transfers between devices  520 us (68%)
  local copies, waits for them, and re-layouts  110 us (14%)
  matrix products  52.3 us (7%)
  loops' own time  27 us (4%)
  other arithmetic  25.5 us (3%)
  starting transfers between devices  17.6 us (2%)
  between operations  13.7 us (2%)
    all_gather x1, waiting for transfers between devices, per_device(): down_full = lax.all_gather(down_weight, 'sp', axis=1, tiled=True)  93.4 us
    all_gather x1, waiting for transfers between devices, per_device(): lax.all_gather(gate_weight, 'sp', axis=0, tiled=True)  87.9 us
    all_gather x1, waiting for transfers between devices, per_device(): lax.all_gather(up_weight, 'sp', axis=0, tiled=True)  84.5 us
    ppermute x7, waiting for transfers between devices, per_device(): lax.ppermute(ring[-1], 'sp', [(dev, (dev + 1) % 8) for dev in range(8)])  57.8 us
    ppermute x12, waiting for transfers between devices, from_partner(): return lax.ppermute(value, axis, pairs)  48.5 us
    psum x1, waiting for transfers between devices, per_device(): lax.psum((jnp.dot(attended_small, output_small, preferred_element_type=jn...  48.5 us
    all_gather x1, waiting for transfers between devices, per_device(): values_first = lax.all_gather(value_small, 'sp', axis=0, tiled=True)  38.1 us
    reduce_scatter x1, waiting for transfers between devices, per_device(): lax.psum_scatter(jnp.dot(hidden, down_full, preferred_element_type=jnp.fl...  29.5 us
  transfers between devices with their start and end apart: 28, of which 22 were waited for; matrix products, arithmetic and copies ran while one was open for 21% of the time, Pallas kernels for 0%

profile of v1, /device:TPU:0, one launch (start us, length us, event | category | flops | bytes accessed | tf_op | source)
XLA Modules:
  0.0 766.2 jit_solution(10103897854299725620)
XLA Ops:
  13.8 9.4 %collective-permute-done = bf16[512,2,128]{2,0,1:T(8,128)(2,1)S(1)} collective-permute-done((bf16[512,2,128]{2,0,1:T(8,128)(2,1)S(1)}, bf16[512,2,128]{2,0,1:T(8,128)(2,1)S(1)}, u32[]{:S(2)}, u32[]{:S(2)}) %collective-permute-start) | collective-permute-done | bytes 262176 | tf_op jit(solution)/shard_map/ppermute | solution.py:119
  23.2 16.6 %collective-permute-done.1 = bf16[512,2,128]{2,0,1:T(8,128)(2,1)S(1)} collective-permute-done((bf16[512,2,128]{2,0,1:T(8,128)(2,1)S(1)}, bf16[512,2,128]{2,0,1:T(8,128)(2,1)S(1)}, u32[]{:S(2)}, u32[]{:S(2)}) %collective-permute-start.1) | collective-permute-done | bytes 262176 | tf_op jit(solution)/shard_map/ppermute | solution.py:119
  39.8 14.0 %collective-permute-done.2 = bf16[512,2,128]{2,0,1:T(8,128)(2,1)S(1)} collective-permute-done((bf16[512,2,128]{2,0,1:T(8,128)(2,1)S(1)}, bf16[512,2,128]{2,0,1:T(8,128)(2,1)S(1)}, u32[]{:S(2)}, u32[]{:S(2)}) %collective-permute-start.2) | collective-permute-done | bytes 262176 | tf_op jit(solution)/shard_map/ppermute | solution.py:119
  54.4 12.1 %collective-permute-done.3 = bf16[512,2,128]{2,0,1:T(8,128)(2,1)S(1)} collective-permute-done((bf16[512,2,128]{2,0,1:T(8,128)(2,1)S(1)}, bf16[512,2,128]{2,0,1:T(8,128)(2,1)S(1)}, u32[]{:S(2)}, u32[]{:S(2)}) %collective-permute-start.3) | collective-permute-done | bytes 262176 | tf_op jit(solution)/shard_map/ppermute | solution.py:119
  66.5 8.6 %collective-permute-done.10 = bf16[256,2,256]{0,2,1:T(8,128)(2,1)S(1)} collective-permute-done((bf16[256,2,256]{0,2,1:T(8,128)(2,1)S(1)}, bf16[256,2,256]{0,2,1:T(8,128)(2,1)S(1)}, u32[]{:S(2)}, u32[]{:S(2)}) %collective-permute-start.10) | collective-permute-done | bytes 262176 | tf_op jit(solution)/shard_map/ppermute | solution.py:16
  75.1 4.7 collective-permute-done.4
  80.1 7.4 collective-permute-done.7
  87.5 3.2 collective-permute-start.12
  95.6 19.1 %collective-permute-done.9 = bf16[256,2,128]{2,1,0:T(2,128)(2,1)S(1)} collective-permute-done((bf16[256,2,128]{2,1,0:T(2,128)(2,1)S(1)}, bf16[256,2,128]{2,1,0:T(2,128)(2,1)S(1)}, u32[]{:S(2)}, u32[]{:S(2)}) %collective-permute-start.9) | collective-permute-done | bytes 131104 | tf_op jit(solution)/shard_map/ppermute | solution.py:16
  122.8 9.7 %reshape.126 = bf16[8,512,2,2,64]{4,3,2,1,0:T(2,128)(2,1)} reshape(bf16[4096,2,128]{2,1,0:T(2,128)(2,1)} %all-gather.10.cloned.1.call-done) | data formatting | bytes 4194304 | tf_op jit(solution)/shard_map/reshape | solution.py:127
  132.5 10.7 %copy.60 = bf16[8,512,2,2,64]{1,4,3,2,0:T(8,128)(2,1)} copy(bf16[8,512,2,2,64]{4,3,2,1,0:T(2,128)(2,1)} %reshape.126) | data formatting | bytes 4194304 | tf_op jit(solution)/shard_map/while | solution.py:154
  143.1 28.9 %all-gather.14.cloned.1.call-done = bf16[4096,2,256]{2,1,0:T(2,128)(2,1)} async-done(((bf16[512,2,256]{2,1,0:T(2,128)(2,1)}), bf16[4096,2,256]{2,1,0:T(2,128)(2,1)}) %all-gather.14.cloned.1.call-update) | async-done | bytes 4194320 | tf_op jit(solution)/shard_map/all_gather | solution.py:115
  172.0 11.7 %reshape.127 = bf16[8,512,2,2,128]{4,3,2,1,0:T(2,128)(2,1)} reshape(bf16[4096,2,256]{2,1,0:T(2,128)(2,1)} %all-gather.14.cloned.1.call-done) | data formatting | bytes 8388608 | tf_op jit(solution)/shard_map/reshape | solution.py:128
  183.7 38.1 %all-gather.12.cloned.1.call-done = bf16[4096,2,128]{2,0,1:T(8,128)(2,1)} async-done(((bf16[512,2,128]{2,0,1:T(8,128)(2,1)}), bf16[4096,2,128]{2,0,1:T(8,128)(2,1)}) %all-gather.12.cloned.1.call-update) | async-done | bytes 2097168 | tf_op jit(solution)/shard_map/all_gather | solution.py:116
  225.2 126.4 %while.32 = (s32[]{:T(128)}, f32[2,2,256]{2,1,0:T(2,128)S(1)}, f32[2,2,256]{2,1,0:T(2,128)S(1)}, f32[2,2,256,128]{3,2,1,0:T(8,128)}, f32[2,2,256]{2,1,0:T(2,128)...) while((s32[]{:T(128)}, f32[2,2,256]{2,1,0:T(2,128)S(1)}, ...), condition=%wide.region_13.14_spmd, body=%wide.region_0.13_spmd.sunk | while | flops 968106496 | bytes 58991568 | solution.py:154
  232.7 5.8 conditional.5
  240.4 5.8 conditional.4
  253.4 5.8 conditional.5
  268.5 5.8 conditional.5
  283.5 5.8 conditional.5
  298.6 5.8 conditional.5
  313.6 5.8 conditional.5
  328.7 5.8 conditional.5
  343.7 5.8 conditional.5
  385.9 48.5 %all-reduce.2.cloned.1.call-done = bf16[512,2048]{1,0:T(8,128)(2,1)} async-done(((bf16[512,2048]{1,0:T(8,128)(2,1)}), bf16[512,2048]{1,0:T(8,128)(2,1)}) %all-reduce.2.cloned.1.call-update) | async-done | bytes 2097168 | tf_op jit(solution)/shard_map/psum | solution.py:166
  434.3 3.1 fusion.48
  440.9 87.9 %all-gather.16.cloned.1.call-done = bf16[2048,1408]{1,0:T(8,128)(2,1)} async-done(((bf16[256,1408]{1,0:T(8,128)(2,1)}), bf16[2048,1408]{1,0:T(8,128)(2,1)}) %all-gather.16.cloned.1.call-update) | async-done | bytes 5767184 | tf_op jit(solution)/shard_map/all_gather | solution.py:179
  528.8 8.2 %fusion.72 = f32[512,1408]{1,0:T(8,128)} fusion(bf16[512,2048]{1,0:T(8,128)(2,1)} %multiply_convert_fusion, bf16[2048,1408]{1,0:T(8,128)(2,1)} %all-gather.16.cloned.1.call-done), kind=kOutput, calls=%fused_computation.148 | convolution fusion | flops 2952790016 | bytes 10747904 | tf_op jit(solution)/shard_map/dot_general | solution.py:177
  537.0 84.5 %all-gather.18.cloned.1.call-done = bf16[2048,1408]{1,0:T(8,128)(2,1)} async-done(((bf16[256,1408]{1,0:T(8,128)(2,1)}), bf16[2048,1408]{1,0:T(8,128)(2,1)}) %all-gather.18.cloned.1.call-update) | async-done | bytes 5767184 | tf_op jit(solution)/shard_map/all_gather | solution.py:184
  621.5 93.4 %all-gather.20.cloned.1.call-done = bf16[1408,2048]{1,0:T(8,128)(2,1)} async-done(((bf16[1408,256]{1,0:T(8,128)(2,1)}), bf16[1408,2048]{1,0:T(8,128)(2,1)}) %all-gather.20.cloned.1.call-update) | async-done | bytes 5767184 | tf_op jit(solution)/shard_map/all_gather | solution.py:187
  714.9 13.2 %convolution_convert_fusion = bf16[512,2048]{1,0:T(8,128)(2,1)} fusion(bf16[1408,2048]{1,0:T(8,128)(2,1)} %all-gather.20.cloned.1.call-done, bf16[512,2048]{1,0:T(8,128)(2,1)S(1)} %copy-done.3, bf16[2048,1408]{1,0:T(8,128)(2,1)} %all-gather.18.cloned.1.call-done, f32[512,1408]{1,0:T(8,128)} %fusion.72), kind=kOutput, calls=%fused_computation.79 | convolution fusion | flops 5910953984 | bytes 18612224 | tf_op jit(solution)/shard_map/dot_general | solution.py:190
  728.1 29.5 %reduce-scatter.2.cloned.1.call-done = bf16[128,2048]{1,0:T(8,128)(2,1)} async-done(((bf16[512,2048]{1,0:T(8,128)(2,1)}), bf16[128,2048]{1,0:T(8,128)(2,1)}) %reduce-scatter.2.cloned.1.call-update) | async-done | bytes 524304 | tf_op jit(solution)/shard_map/reduce_scatter | solution.py:189
  (400 shorter events, 163.2 us)
Async XLA Ops:
  6.5 372.2 %copy-start = (bf16[256,2048]{1,0:T(8,128)(2,1)S(1)}, bf16[256,2048]{1,0:T(8,128)(2,1)}, u32[]{:S(2)}) copy-start(bf16[256,2048]{1,0:T(8,128)(2,1)} %param.33) | copy-start | bytes 3145732
  6.5 73.3 %copy-start.19 = (bf16[512,2,128]{2,1,0:T(2,128)(2,1)S(1)}, bf16[512,2,128]{2,1,0:T(2,128)(2,1)}, u32[]{:S(2)}) copy-start(bf16[512,2,128]{2,1,0:T(2,128)(2,1)} %param.23) | copy-start | bytes 786436
  6.5 116.3 %all-gather.10.cloned.1.call-start = ((), (), s32[]{:S(2)}) async-start(), calls=%async_computation.2 | async-start | bytes 2359296 | tf_op jit(solution)/shard_map/all_gather | solution.py:114
  7.3 164.7 %all-gather.14.cloned.1.call-start = ((), (), s32[]{:S(2)}) async-start(), calls=%async_computation.4 | async-start | bytes 4718592 | tf_op jit(solution)/shard_map/all_gather | solution.py:115
  8.0 213.8 %all-gather.12.cloned.1.call-start = ((), (), s32[]{:S(2)}) async-start(), calls=%async_computation.3 | async-start | bytes 2359296 | tf_op jit(solution)/shard_map/all_gather | solution.py:116
  9.8 376.1 %all-gather.8.cloned.1.call-start = ((), (), s32[]{:S(2)}) async-start(), calls=%async_computation.1 | async-start | bytes 2621440 | tf_op jit(solution)/shard_map/all_gather | solution.py:88
  10.8 12.4 %collective-permute-start = (bf16[512,2,128]{2,0,1:T(8,128)(2,1)S(1)}, bf16[512,2,128]{2,0,1:T(8,128)(2,1)S(1)}, u32[]{:S(2)}, u32[]{:S(2)}) collective-permute-start(bf16[512,2,128]{2,0,1:T(8,128)(2,1)S(1)} %copy.53), channel_id=1, source_target_pairs={{0,4},{4,8},{8,12},{12,16},{16,20},{20,24},{24,28},{28,0},{1,5},{5... | collective-permute-start | bytes 786440 | tf_op jit(solution)/shard_map/ppermute | solution.py:119
  23.2 16.6 %collective-permute-start.1 = (bf16[512,2,128]{2,0,1:T(8,128)(2,1)S(1)}, bf16[512,2,128]{2,0,1:T(8,128)(2,1)S(1)}, u32[]{:S(2)}, u32[]{:S(2)}) collective-permute-start(bf16[512,2,128]{2,0,1:T(8,128)(2,1)S(1)} %collective-permute-done), channel_id=1, source_target_pairs={{0,4},{4,8},{8,12},{12,16},{16,20},{20,24},{24,28},{28,0},{1,5},{5... | collective-permute-start | bytes 786440 | tf_op jit(solution)/shard_map/ppermute | solution.py:119
  39.8 14.0 %collective-permute-start.2 = (bf16[512,2,128]{2,0,1:T(8,128)(2,1)S(1)}, bf16[512,2,128]{2,0,1:T(8,128)(2,1)S(1)}, u32[]{:S(2)}, u32[]{:S(2)}) collective-permute-start(bf16[512,2,128]{2,0,1:T(8,128)(2,1)S(1)} %collective-permute-done.1), channel_id=1, source_target_pairs={{0,4},{4,8},{8,12},{12,16},{16,20},{20,24},{24,28},{28,0},{1,5},{5... | collective-permute-start | bytes 786440 | tf_op jit(solution)/shard_map/ppermute | solution.py:119
  53.8 12.7 %collective-permute-start.3 = (bf16[512,2,128]{2,0,1:T(8,128)(2,1)S(1)}, bf16[512,2,128]{2,0,1:T(8,128)(2,1)S(1)}, u32[]{:S(2)}, u32[]{:S(2)}) collective-permute-start(bf16[512,2,128]{2,0,1:T(8,128)(2,1)S(1)} %collective-permute-done.2), channel_id=1, source_target_pairs={{0,4},{4,8},{8,12},{12,16},{16,20},{20,24},{24,28},{28,0},{1,5},{5... | collective-permute-start | bytes 786440 | tf_op jit(solution)/shard_map/ppermute | solution.py:119
  54.4 20.8 %collective-permute-start.10 = (bf16[256,2,256]{0,2,1:T(8,128)(2,1)S(1)}, bf16[256,2,256]{0,2,1:T(8,128)(2,1)S(1)}, u32[]{:S(2)}, u32[]{:S(2)}) collective-permute-start(bf16[256,2,256]{0,2,1:T(8,128)(2,1)S(1)} %copy.86), channel_id=1, source_target_pairs={{0,4},{4,0},{8,12},{12,8},{16,20},{20,16},{24,28},{28,24},{1,5},{5... | collective-permute-start | bytes 786440 | tf_op jit(solution)/shard_map/ppermute | solution.py:16
  66.5 13.3 %collective-permute-start.4 = (bf16[512,2,128]{2,0,1:T(8,128)(2,1)S(1)}, bf16[512,2,128]{2,0,1:T(8,128)(2,1)S(1)}, u32[]{:S(2)}, u32[]{:S(2)}) collective-permute-start(bf16[512,2,128]{2,0,1:T(8,128)(2,1)S(1)} %collective-permute-done.3), channel_id=1, source_target_pairs={{0,4},{4,8},{8,12},{12,16},{16,20},{20,24},{24,28},{28,0},{1,5},{5... | collective-permute-start | bytes 786440 | tf_op jit(solution)/shard_map/ppermute | solution.py:119
  75.1 12.4 %collective-permute-start.11 = (bf16[256,2,256]{0,2,1:T(8,128)(2,1)S(1)}, bf16[256,2,256]{0,2,1:T(8,128)(2,1)}, u32[]{:S(2)}, u32[]{:S(2)}) collective-permute-start(bf16[256,2,256]{0,2,1:T(8,128)(2,1)S(1)} %collective-permute-done.10), channel_id=1, source_target_pairs={{0,8},{4,12},{8,0},{12,4},{16,24},{20,28},{24,16},{28,20},{1,9},{5... | collective-permute-start | bytes 786440 | tf_op jit(solution)/shard_map/ppermute | solution.py:16
  79.8 12.1 %collective-permute-start.5 = (bf16[512,2,128]{2,0,1:T(8,128)(2,1)S(1)}, bf16[512,2,128]{2,0,1:T(8,128)(2,1)}, u32[]{:S(2)}, u32[]{:S(2)}) collective-permute-start(bf16[512,2,128]{2,0,1:T(8,128)(2,1)S(1)} %collective-permute-done.4), channel_id=1, source_target_pairs={{0,4},{4,8},{8,12},{12,16},{16,20},{20,24},{24,28},{28,0},{1,5},{5... | collective-permute-start | bytes 786440 | tf_op jit(solution)/shard_map/ppermute | solution.py:119
  80.0 7.5 collective-permute-start.7
  87.5 6.8 collective-permute-start.8
  87.5 27.3 %collective-permute-start.12 = (bf16[256,2,256]{0,2,1:T(8,128)(2,1)}, bf16[256,2,256]{0,2,1:T(8,128)(2,1)S(1)}, u32[]{:S(2)}, u32[]{:S(2)}) collective-permute-start(bf16[256,2,256]{0,2,1:T(8,128)(2,1)} %collective-permute-done.11), channel_id=1, source_target_pairs={{0,16},{4,20},{8,24},{12,28},{16,0},{20,4},{24,8},{28,12},{1,17},{... | collective-permute-start | bytes 786440 | tf_op jit(solution)/shard_map/ppermute | solution.py:16
  91.9 24.8 %collective-permute-start.6 = (bf16[512,2,128]{2,0,1:T(8,128)(2,1)}, bf16[512,2,128]{2,0,1:T(8,128)(2,1)}, u32[]{:S(2)}, u32[]{:S(2)}) collective-permute-start(bf16[512,2,128]{2,0,1:T(8,128)(2,1)} %collective-permute-done.5), channel_id=1, source_target_pairs={{0,4},{4,8},{8,12},{12,16},{16,20},{20,24},{24,28},{28,0},{1,5},{5... | collective-permute-start | bytes 786440 | tf_op jit(solution)/shard_map/ppermute | solution.py:119
  94.3 20.4 %collective-permute-start.9 = (bf16[256,2,128]{2,1,0:T(2,128)(2,1)S(1)}, bf16[256,2,128]{2,1,0:T(2,128)(2,1)S(1)}, u32[]{:S(2)}, u32[]{:S(2)}) collective-permute-start(bf16[256,2,128]{2,1,0:T(2,128)(2,1)S(1)} %collective-permute-done.8), channel_id=1, source_target_pairs={{0,16},{4,20},{8,24},{12,28},{16,0},{20,4},{24,8},{28,12},{1,17},{... | collective-permute-start | bytes 393224 | tf_op jit(solution)/shard_map/ppermute | solution.py:16
  95.0 339.3 %all-reduce.2.cloned.1.call-start = ((), (), s32[]{:S(2)}) async-start(), calls=%async_computation.5 | async-start | bytes 4194304 | tf_op jit(solution)/shard_map/psum | solution.py:166
  359.8 5.0 collective-permute-start.16
  360.3 6.5 collective-permute-start.13
  364.9 6.2 collective-permute-start.17
  366.8 6.6 collective-permute-start.14
  371.1 7.7 %collective-permute-start.18 = (bf16[256,256]{0,1:T(8,128)(2,1)S(1)}, bf16[256,256]{0,1:T(8,128)(2,1)S(1)}, u32[]{:S(2)}, u32[]{:S(2)}) collective-permute-start(bf16[256,256]{0,1:T(8,128)(2,1)S(1)} %collective-permute-done.17), channel_id=1, source_target_pairs={{0,16},{4,20},{8,24},{12,28},{16,0},{20,4},{24,8},{28,12},{1,17},{... | collective-permute-start | bytes 393224 | tf_op jit(solution)/shard_map/ppermute | solution.py:16
  373.4 8.2 %collective-permute-start.15 = (bf16[256,256]{0,1:T(8,128)(2,1)S(1)}, bf16[256,256]{0,1:T(8,128)(2,1)S(1)}, u32[]{:S(2)}, u32[]{:S(2)}) collective-permute-start(bf16[256,256]{0,1:T(8,128)(2,1)S(1)} %collective-permute-done.14), channel_id=1, source_target_pairs={{0,16},{4,20},{8,24},{12,28},{16,0},{20,4},{24,8},{28,12},{1,17},{... | collective-permute-start | bytes 393224 | tf_op jit(solution)/shard_map/ppermute | solution.py:16
  383.7 145.1 %all-gather.16.cloned.1.call-start = ((), (), s32[]{:S(2)}) async-start(), calls=%async_computation.6 | async-start | bytes 6488064 | tf_op jit(solution)/shard_map/all_gather | solution.py:179
  384.3 237.2 %all-gather.18.cloned.1.call-start = ((), (), s32[]{:S(2)}) async-start(), calls=%async_computation.7 | async-start | bytes 6488064 | tf_op jit(solution)/shard_map/all_gather | solution.py:184
  385.0 329.8 %all-gather.20.cloned.1.call-start = ((), (), s32[]{:S(2)}) async-start(), calls=%async_computation.8 | async-start | bytes 6488064 | tf_op jit(solution)/shard_map/all_gather | solution.py:187
  385.8 371.8 %reduce-scatter.2.cloned.1.call-start = ((), (), s32[]{:S(2)}) async-start(), calls=%async_computation.9 | async-start | bytes 2621440 | tf_op jit(solution)/shard_map/reduce_scatter | solution.py:189
  385.8 51.6 %copy-start.1 = (bf16[512,2048]{1,0:T(8,128)(2,1)S(1)}, bf16[512,2048]{1,0:T(8,128)(2,1)}, u32[]{:S(2)}) copy-start(bf16[512,2048]{1,0:T(8,128)(2,1)} %all-gather.8.cloned.1.call-done) | copy-start | bytes 6291460
  440.9 273.9 %copy-start.3 = (bf16[512,2048]{1,0:T(8,128)(2,1)S(1)}, bf16[512,2048]{1,0:T(8,128)(2,1)}, u32[]{:S(2)}) copy-start(bf16[512,2048]{1,0:T(8,128)(2,1)} %multiply_convert_fusion) | copy-start | bytes 6291460
  (49 other events, 115.6 us)
Sparse Core Ops, SparseCore 0:
  9.5 76.7 all-gather.9
  88.4 83.5 all-gather.13
  174.2 47.5 all-gather.11
  223.2 21.0 all-gather.7
  383.8 50.4 all-reduce.1
  436.4 92.3 all-gather.15
  530.9 90.4 all-gather.17
  623.5 91.2 all-gather.19
  728.2 29.3 reduce-scatter.1
